TPU v7x, 32 devices: a whole 2x2x4 slice. The times are simulated.
32 devices in a mesh: fs: 8 (over z, y), tp: 4 (over x, core).
Axes of the slice: x: 2, y: 2, z: 4, core: 2. Of those that a mesh axis runs over, the one named last changes fastest.
Arguments:
- tokens: bfloat16 [8192, 2048], P('fs', 'tp'), may hold values from -6 to 6
- norm_gain: float32 [2048], P('fs'), may hold values from 0.1 to 1.9
- up_master: float32 [2048, 4096], P('fs', 'tp'), may hold values from -0.125 to 0.125
- down_master: float32 [4096, 2048], P('fs', 'tp'), may hold values from -0.09375 to 0.09375
Outputs:
- mixed: bfloat16 [8192, 2048], P('fs', 'tp')
- up_ready: bfloat16 [2048, 4096], P(None, 'tp')
- down_ready: bfloat16 [4096, 2048], P('tp')
All inputs are finite; a program needn't handle non-finite values.
Results may differ from a plain program's by a relative error of at most 0.0095.
Values may be sent and summed in bfloat16 or wider, within the bound.
A program may use at most 128 MiB of HBM per device.

v0:
```python
import jax
import jax.numpy as jnp
from jax import lax
from jax.sharding import PartitionSpec as P


def shards(tokens, norm_gain, up_master, down_master):
    up_local = (norm_gain[:, None] * up_master).astype(jnp.bfloat16)
    up_ready = lax.all_gather(up_local, "fs", axis=0, tiled=True)
    down_local = down_master.astype(jnp.bfloat16)
    gathered = lax.all_gather(down_local, "fs", axis=0, tiled=True)
    down_ready = lax.all_to_all(gathered, "tp", split_axis=0, concat_axis=1, tiled=True)
    features = lax.all_gather(tokens, "tp", axis=1, tiled=True)
    values = features.astype(jnp.float32)
    mean_square = jnp.mean(values * values, axis=-1, keepdims=True)
    normed = (values * lax.rsqrt(mean_square + 1e-06)).astype(jnp.bfloat16)
    before = jnp.dot(normed, up_ready, preferred_element_type=jnp.float32)
    hidden = jnp.square(jax.nn.relu(before)).astype(jnp.bfloat16)
    partial_value = jnp.dot(hidden, down_ready, preferred_element_type=jnp.float32)
    mixed = lax.psum_scatter(
        partial_value.astype(jnp.bfloat16), "tp", scatter_dimension=1, tiled=True
    )
    return (mixed, up_ready, down_ready)


def solution(mesh):
    return jax.shard_map(
        shards,
        mesh=mesh,
        in_specs=(P("fs", "tp"), P("fs"), P("fs", "tp"), P("fs", "tp")),
        out_specs=(P("fs", "tp"), P(None, "tp"), P("tp", None)),
        check_vma=False,
    )
```

profile of v0, /device:TPU:0, one launch (start us, length us, event | category | flops | bytes accessed | tf_op | source)
XLA Modules:
  0.0 287.9 jit_solution(17428654618168584598)
XLA Ops:
  7.2 0.0 all-gather.8.cloned.1.call-start
  7.2 2.1 convert_element_type.22
  9.3 0.0 all-gather.8.cloned.1.call-update
  9.3 0.0 all-gather.4.cloned.1.call-start
  9.4 0.7 all-gather.4.cloned.1.call-update
  10.1 0.0 all-gather.6.cloned.1.call-start
  10.1 2.1 multiply_convert_fusion.2
  12.3 0.0 all-gather.6.cloned.1.call-update
  12.3 73.9 %all-gather.8.cloned.1.call-done = bf16[4096,512]{1,0:T(8,128)(2,1)} async-done(((bf16[512,512]{1,0:T(8,128)(2,1)}), bf16[4096,512]{1,0:T(8,128)(2,1)}) %all-gather.8.cloned.1.call-update) | async-done | bytes 4194320 | tf_op jit(solution)/shard_map/all_gather | solution.py:11
  86.2 4.9 %all-to-all-start = ((bf16[4,1024,512]{2,1,0:T(8,128)(2,1)}), bf16[4,1024,512]{2,1,0:T(8,128)(2,1)}, u32[]{:S(2)}, u32[]{:S(2)}) async-start(bf16[4,1024,512]{2,1,0:T(8,128)(2,1)} %bitcast.8), calls=%async_computation | async-start | bytes 8388608 | tf_op jit(solution)/shard_map/all_to_all | solution.py:12
  91.1 0.0 reduce-scatter.2.cloned.1.call-start
  91.2 52.2 %all-gather.4.cloned.1.call-done = bf16[1024,2048]{1,0:T(8,128)(2,1)} async-done(((bf16[1024,512]{1,0:T(8,128)(2,1)}), bf16[1024,2048]{1,0:T(8,128)(2,1)}) %all-gather.4.cloned.1.call-update) | async-done | bytes 4194320 | tf_op jit(solution)/shard_map/all_gather | solution.py:13
  143.4 3.1 %fusion = f32[1024]{0:T(1024)S(1)} fusion(bf16[1024,2048]{1,0:T(8,128)(2,1)} %all-gather.4.cloned.1.call-done), kind=kLoop, calls=%fused_computation.2 | loop fusion | flops 6290432 | bytes 4198400 | tf_op jit(solution)/shard_map/reduce_sum | solution.py:15
  146.5 15.3 %all-to-all-done = bf16[4,1024,512]{2,1,0:T(8,128)(2,1)} async-done(((bf16[4,1024,512]{2,1,0:T(8,128)(2,1)}), bf16[4,1024,512]{2,1,0:T(8,128)(2,1)}, u32[]{:S(2)}, u32[]{:S(2)}) %all-to-all-start) | async-done | bytes 4194336 | tf_op jit(solution)/shard_map/all_to_all | solution.py:12
  161.8 6.2 %copy.8 = bf16[4,1024,512]{1,2,0:T(8,128)(2,1)} copy(bf16[4,1024,512]{2,1,0:T(8,128)(2,1)} %all-to-all-done) | data formatting | bytes 8388608 | tf_op jit(solution)/shard_map/all_to_all | solution.py:12
  168.0 50.9 %all-gather.6.cloned.1.call-done = bf16[2048,1024]{1,0:T(8,128)(2,1)} async-done(((bf16[256,1024]{1,0:T(8,128)(2,1)}), bf16[2048,1024]{1,0:T(8,128)(2,1)}) %all-gather.6.cloned.1.call-update) | async-done | bytes 4194320 | tf_op jit(solution)/shard_map/all_gather | solution.py:9
  218.9 14.7 %convolution_convert_fusion = bf16[1024,2048]{1,0:T(8,128)(2,1)} fusion(bf16[1024,2048]{0,1:T(8,128)(2,1)} %bitcast.6, bf16[2048,1024]{1,0:T(8,128)(2,1)} %all-gather.6.cloned.1.call-done, bf16[1024,2048]{1,0:T(8,128)(2,1)} %all-gather.4.cloned.1.call-done, f32[1024]{0:T(1024)S(1)} %add_rsqrt_fusion), kind=kOutput, calls=%fused_computation.7 | convolution fusion | flops 8601468928 | bytes 16781312 | tf_op jit(solution)/shard_map/dot_general | solution.py:19
  233.6 0.0 reduce-scatter.2.cloned.1.call-update
  233.6 6.5 %copy.9 = bf16[1024,2048]{1,0:T(8,128)(2,1)} copy(bf16[1024,2048]{0,1:T(8,128)(2,1)} %bitcast.7) | data formatting | bytes 8388608
  240.1 36.6 %reduce-scatter.2.cloned.1.call-done = bf16[1024,512]{1,0:T(8,128)(2,1)} async-done(((bf16[1024,2048]{1,0:T(8,128)(2,1)}), bf16[1024,512]{1,0:T(8,128)(2,1)}) %reduce-scatter.2.cloned.1.call-update) | async-done | bytes 1048592 | tf_op jit(solution)/shard_map/reduce_scatter | solution.py:20
  276.7 4.6 %copy.11 = bf16[2048,1024]{1,0:T(8,128)(2,1)} copy(bf16[2048,1024]{1,0:T(8,128)(2,1)} %all-gather.6.cloned.1.call-done) | data formatting | bytes 8388608
  (1 shorter events, 0.0 us)
Async XLA Ops:
  7.2 79.1 %all-gather.8.cloned.1.call-start = ((), (), s32[]{:S(2)}) async-start(), calls=%async_computation.4 | async-start | bytes 4718592 | tf_op jit(solution)/shard_map/all_gather | solution.py:11
  9.3 134.1 %all-gather.4.cloned.1.call-start = ((), (), s32[]{:S(2)}) async-start(), calls=%async_computation.2 | async-start | bytes 5242880 | tf_op jit(solution)/shard_map/all_gather | solution.py:13
  10.1 208.8 %all-gather.6.cloned.1.call-start = ((), (), s32[]{:S(2)}) async-start(), calls=%async_computation.3 | async-start | bytes 4718592 | tf_op jit(solution)/shard_map/all_gather | solution.py:9
  86.2 75.6 %all-to-all-start = ((bf16[4,1024,512]{2,1,0:T(8,128)(2,1)}), bf16[4,1024,512]{2,1,0:T(8,128)(2,1)}, u32[]{:S(2)}, u32[]{:S(2)}) async-start(bf16[4,1024,512]{2,1,0:T(8,128)(2,1)} %bitcast.8), calls=%async_computation | async-start | bytes 8388608 | tf_op jit(solution)/shard_map/all_to_all | solution.py:12
  91.1 185.6 %reduce-scatter.2.cloned.1.call-start = ((), (), s32[]{:S(2)}) async-start(), calls=%async_computation.5 | async-start | bytes 5242880 | tf_op jit(solution)/shard_map/reduce_scatter | solution.py:20
Sparse Core Ops, SparseCore 0:
  10.7 75.5 all-gather.7
  87.8 55.5 all-gather.3
  146.1 72.7 all-gather.5
  233.7 42.9 reduce-scatter.1
where the time goes:
time: 288 us
  waiting for transfers between devices  230 us (80%)
  local copies, waits for them, and re-layouts  17.3 us (6%)
  matrix products  14.7 us (5%)
  between operations  13.8 us (5%)
  other arithmetic  7.31 us (3%)
  starting transfers between devices  5.06 us (2%)
    all_gather x1, waiting for transfers between devices, shards(): gathered = lax.all_gather(down_local, 'fs', axis=0, tiled=True)  73.9 us
    all_gather x1, waiting for transfers between devices, shards(): features = lax.all_gather(tokens, 'tp', axis=1, tiled=True)  52.2 us
    all_gather x1, waiting for transfers between devices, shards(): up_ready = lax.all_gather(up_local, 'fs', axis=0, tiled=True)  50.9 us
    reduce_scatter x1, waiting for transfers between devices, shards(): lax.psum_scatter(partial_value.astype(jnp.bfloat16), 'tp', scatter_dimens...  36.6 us
    all_to_all x1, waiting for transfers between devices, shards(): lax.all_to_all(gathered, 'tp', split_axis=0, concat_axis=1, tiled=True)  15.3 us
    dot_general x1, matrix products, shards(): jnp.dot(hidden, down_ready, preferred_element_type=jnp.float32)  14.7 us
    unnamed x2, local copies, waits for them, and re-layouts  11.1 us
    all_to_all x1, local copies, waits for them, and re-layouts, shards(): lax.all_to_all(gathered, 'tp', split_axis=0, concat_axis=1, tiled=True)  6.21 us
  transfers between devices with their start and end apart: 5, of which 5 were waited for; matrix products, arithmetic and copies ran while one was open for 6% of the time, Pallas kernels for 0%

commit v1 on v0

--- a/solution.py
+++ b/solution.py
@@ -6,7 +6,12 @@
 
 def shards(tokens, norm_gain, up_master, down_master):
     up_local = (norm_gain[:, None] * up_master).astype(jnp.bfloat16)
-    up_ready = lax.all_gather(up_local, "fs", axis=0, tiled=True)
+    ring = [up_local]
+    for hop in range(7):
+        ring.append(lax.ppermute(ring[-1], "fs", [(dev, (dev + 1) % 8) for dev in range(8)]))
+    up_ready = jnp.roll(
+        jnp.concatenate(ring[::-1], axis=0), (lax.axis_index("fs") + 1) * ring[0].shape[0], axis=0
+    )
     down_local = down_master.astype(jnp.bfloat16)
     gathered = lax.all_gather(down_local, "fs", axis=0, tiled=True)
     down_ready = lax.all_to_all(gathered, "tp", split_axis=0, concat_axis=1, tiled=True)

time: 288 us -> 276 us (0.958)
  waiting for transfers between devices: 230 us -> 210 us
  local copies, waits for them, and re-layouts: 17.3 us -> 21.7 us
  starting transfers between devices: 5.06 us -> 8.48 us
    ppermute x0 -> x7, waiting for transfers between devices: none -> 137 us  [shards(): lax.ppermute(ring[-1], 'fs', [(dev, (dev + 1) % 8) for dev in range(8)])]
    all_gather x1, waiting for transfers between devices: 73.9 us -> 0.01 us  [shards(): gathered = lax.all_gather(down_local, 'fs', axis=0, tiled=True)]
    all_gather x1, waiting for transfers between devices: 52.2 us -> 0.01 us  [shards(): features = lax.all_gather(tokens, 'tp', axis=1, tiled=True)]
    all_gather x1 -> x0, waiting for transfers between devices: 50.9 us -> none  [shards(): up_ready = lax.all_gather(up_local, 'fs', axis=0, tiled=True)]
    all_to_all x1, waiting for transfers between devices: 15.3 us -> 32.5 us  [shards(): lax.all_to_all(gathered, 'tp', split_axis=0, concat_axis=1, tiled=True)]
    ppermute x0 -> x7, starting transfers between devices: none -> 3.4 us  [shards(): lax.ppermute(ring[-1], 'fs', [(dev, (dev + 1) % 8) for dev in range(8)])]
    unnamed x2 -> x23, local copies, waits for them, and re-layouts: 11.1 us -> 13 us
  transfers between devices with their start and end apart: 5 -> 11, of which waited for: 5 -> 9; matrix products, arithmetic and copies ran while one was open for 6% -> 7% of each run, Pallas kernels for 0% -> 0%
where the time goes in v1:
time: 276 us; the launch traced here: 275 us
  waiting for transfers between devices  210 us (76%)
  local copies, waits for them, and re-layouts  21.7 us (8%)
  matrix products  14.7 us (5%)
  between operations  13.9 us (5%)
  starting transfers between devices  8.48 us (3%)
  other arithmetic  6.84 us (2%)
    ppermute x7, waiting for transfers between devices, shards(): lax.ppermute(ring[-1], 'fs', [(dev, (dev + 1) % 8) for dev in range(8)])  137 us
    reduce_scatter x1, waiting for transfers between devices, shards(): lax.psum_scatter(partial_value.astype(jnp.bfloat16), 'tp', scatter_dimens...  39.2 us
    all_to_all x1, waiting for transfers between devices, shards(): lax.all_to_all(gathered, 'tp', split_axis=0, concat_axis=1, tiled=True)  32.5 us
    dot_general x1, matrix products, shards(): jnp.dot(hidden, down_ready, preferred_element_type=jnp.float32)  14.7 us
    unnamed x23, local copies, waits for them, and re-layouts  13 us
    all_to_all x1, local copies, waits for them, and re-layouts, shards(): lax.all_to_all(gathered, 'tp', split_axis=0, concat_axis=1, tiled=True)  6.31 us
  transfers between devices with their start and end apart: 11, of which 9 were waited for; matrix products, arithmetic and copies ran while one was open for 7% of the time, Pallas kernels for 0%

profile of v1, /device:TPU:0, one launch (start us, length us, event | category | flops | bytes accessed | tf_op | source)
XLA Modules:
  0.0 275.4 jit_solution(557496342218837508)
XLA Ops:
  7.2 0.0 all-gather.5.cloned.1.call-start
  7.2 2.1 convert_element_type.22
  9.3 0.0 all-gather.5.cloned.1.call-update
  9.3 0.0 all-gather.3.cloned.1.call-start
  9.4 0.7 all-gather.3.cloned.1.call-update
  10.1 1.4 multiply_convert_fusion.2
  11.5 3.0 %collective-permute-start = (bf16[256,1024]{1,0:T(8,128)(2,1)S(1)}, bf16[256,1024]{1,0:T(8,128)(2,1)S(1)}, u32[]{:S(2)}, u32[]{:S(2)}) collective-permute-start(bf16[256,1024]{1,0:T(8,128)(2,1)S(1)} %multiply_convert_fusion.2), channel_id=1, source_target_pairs={{0,4},{4,8},{8,12},{12,16},{16,20},{20,24},{24,28},{28,0},{1,5},{5... | collective-permute-start | bytes 1572872 | tf_op jit(solution)/shard_map/ppermute | solution.py:11
  14.6 18.2 %collective-permute-done = bf16[256,1024]{1,0:T(8,128)(2,1)S(1)} collective-permute-done((bf16[256,1024]{1,0:T(8,128)(2,1)S(1)}, bf16[256,1024]{1,0:T(8,128)(2,1)S(1)}, u32[]{:S(2)}, u32[]{:S(2)}) %collective-permute-start) | collective-permute-done | bytes 524320 | tf_op jit(solution)/shard_map/ppermute | solution.py:11
  32.7 0.3 collective-permute-start.1
  33.1 24.6 %collective-permute-done.1 = bf16[256,1024]{1,0:T(8,128)(2,1)S(1)} collective-permute-done((bf16[256,1024]{1,0:T(8,128)(2,1)S(1)}, bf16[256,1024]{1,0:T(8,128)(2,1)S(1)}, u32[]{:S(2)}, u32[]{:S(2)}) %collective-permute-start.1) | collective-permute-done | bytes 524320 | tf_op jit(solution)/shard_map/ppermute | solution.py:11
  57.7 26.8 %collective-permute-done.2 = bf16[256,1024]{1,0:T(8,128)(2,1)S(1)} collective-permute-done((bf16[256,1024]{1,0:T(8,128)(2,1)S(1)}, bf16[256,1024]{1,0:T(8,128)(2,1)S(1)}, u32[]{:S(2)}, u32[]{:S(2)}) %collective-permute-start.2) | collective-permute-done | bytes 524320 | tf_op jit(solution)/shard_map/ppermute | solution.py:11
  84.6 26.9 %collective-permute-done.3 = bf16[256,1024]{1,0:T(8,128)(2,1)S(1)} collective-permute-done((bf16[256,1024]{1,0:T(8,128)(2,1)S(1)}, bf16[256,1024]{1,0:T(8,128)(2,1)S(1)}, u32[]{:S(2)}, u32[]{:S(2)}) %collective-permute-start.3) | collective-permute-done | bytes 524320 | tf_op jit(solution)/shard_map/ppermute | solution.py:11
  111.5 18.0 %collective-permute-done.4 = bf16[256,1024]{1,0:T(8,128)(2,1)S(1)} collective-permute-done((bf16[256,1024]{1,0:T(8,128)(2,1)S(1)}, bf16[256,1024]{1,0:T(8,128)(2,1)S(1)}, u32[]{:S(2)}, u32[]{:S(2)}) %collective-permute-start.4) | collective-permute-done | bytes 524320 | tf_op jit(solution)/shard_map/ppermute | solution.py:11
  129.5 0.8 copy-done.1
  130.3 14.2 %collective-permute-done.5 = bf16[256,1024]{1,0:T(8,128)(2,1)} collective-permute-done((bf16[256,1024]{1,0:T(8,128)(2,1)S(1)}, bf16[256,1024]{1,0:T(8,128)(2,1)}, u32[]{:S(2)}, u32[]{:S(2)}) %collective-permute-start.5) | collective-permute-done | bytes 524320 | tf_op jit(solution)/shard_map/ppermute | solution.py:11
  144.5 5.0 %all-to-all-start = ((bf16[4,1024,512]{2,1,0:T(8,128)(2,1)}), bf16[4,1024,512]{2,1,0:T(8,128)(2,1)}, u32[]{:S(2)}, u32[]{:S(2)}) async-start(bf16[4,1024,512]{2,1,0:T(8,128)(2,1)} %bitcast.8), calls=%async_computation | async-start | bytes 8388608 | tf_op jit(solution)/shard_map/all_to_all | solution.py:17
  149.5 0.0 reduce-scatter.2.cloned.1.call-start
  149.6 8.5 %collective-permute-done.6 = bf16[256,1024]{1,0:T(8,128)(2,1)} collective-permute-done((bf16[256,1024]{1,0:T(8,128)(2,1)}, bf16[256,1024]{1,0:T(8,128)(2,1)}, u32[]{:S(2)}, u32[]{:S(2)}) %collective-permute-start.6) | collective-permute-done | bytes 524320 | tf_op jit(solution)/shard_map/ppermute | solution.py:11
  158.1 1.1 constant_dynamic-update-slice_fusion.15
  159.2 1.1 constant_dynamic-update-slice_fusion.14
  160.3 1.1 constant_dynamic-update-slice_fusion.13
  161.6 0.1 constant_dynamic-update-slice_fusion.8
  161.7 1.1 constant_dynamic-update-slice_fusion.7
  162.8 1.1 constant_dynamic-update-slice_fusion.6
  164.1 0.1 constant_dynamic-update-slice_fusion
  164.2 2.5 constant_dynamic-slice_fusion
  166.7 3.1 %fusion = f32[1024]{0:T(1024)S(1)} fusion(bf16[1024,2048]{1,0:T(8,128)(2,1)} %all-gather.3.cloned.1.call-done), kind=kLoop, calls=%fused_computation.2 | loop fusion | flops 6290432 | bytes 4198400 | tf_op jit(solution)/shard_map/reduce_sum | solution.py:20
  169.8 32.5 %all-to-all-done = bf16[4,1024,512]{2,1,0:T(8,128)(2,1)} async-done(((bf16[4,1024,512]{2,1,0:T(8,128)(2,1)}), bf16[4,1024,512]{2,1,0:T(8,128)(2,1)}, u32[]{:S(2)}, u32[]{:S(2)}) %all-to-all-start) | async-done | bytes 4194336 | tf_op jit(solution)/shard_map/all_to_all | solution.py:17
  202.2 6.3 %copy.8 = bf16[4,1024,512]{1,2,0:T(8,128)(2,1)} copy(bf16[4,1024,512]{2,1,0:T(8,128)(2,1)} %all-to-all-done) | data formatting | bytes 8388608 | tf_op jit(solution)/shard_map/all_to_all | solution.py:17
  208.5 14.7 %convolution_convert_fusion = bf16[1024,2048]{1,0:T(8,128)(2,1)} fusion(bf16[1024,2048]{0,1:T(8,128)(2,1)} %bitcast.6, bf16[2048,1024]{1,0:T(8,128)(2,1)} %constant_dynamic-slice_fusion, bf16[1024,2048]{1,0:T(8,128)(2,1)} %all-gather.3.cloned.1.call-done, f32[1024]{0:T(1024)S(1)} %add_rsqrt_fusion), kind=kOutput, calls=%fused_computation.7 | convolution fusion | flops 8601468928 | bytes 16781312 | tf_op jit(solution)/shard_map/dot_general | solution.py:24
  223.3 6.4 %copy.9 = bf16[1024,2048]{1,0:T(8,128)(2,1)} copy(bf16[1024,2048]{0,1:T(8,128)(2,1)} %bitcast.7) | data formatting | bytes 8388608
  229.7 39.2 %reduce-scatter.2.cloned.1.call-done = bf16[1024,512]{1,0:T(8,128)(2,1)} async-done(((bf16[1024,2048]{1,0:T(8,128)(2,1)}), bf16[1024,512]{1,0:T(8,128)(2,1)}) %reduce-scatter.2.cloned.1.call-update) | async-done | bytes 1048592 | tf_op jit(solution)/shard_map/reduce_scatter | solution.py:25
  (25 shorter events, 0.4 us)
Async XLA Ops:
  7.2 137.4 %all-gather.5.cloned.1.call-start = ((), (), s32[]{:S(2)}) async-start(), calls=%async_computation.3 | async-start | bytes 4718592 | tf_op jit(solution)/shard_map/all_gather | solution.py:16
  9.3 157.4 %all-gather.3.cloned.1.call-start = ((), (), s32[]{:S(2)}) async-start(), calls=%async_computation.2 | async-start | bytes 5242880 | tf_op jit(solution)/shard_map/all_gather | solution.py:18
  10.1 151.5 %copy-start = (f32[256,1024]{1,0:T(8,128)S(1)}, f32[256,1024]{1,0:T(8,128)}, u32[]{:S(2)}) copy-start(f32[256,1024]{1,0:T(8,128)} %param.6) | copy-start | bytes 3145732
  10.1 151.5 %copy-start.3 = (f32[256]{0:T(256)S(1)}, f32[256]{0:T(256)}, u32[]{:S(2)}) copy-start(f32[256]{0:T(256)} %param.5) | copy-start | bytes 3076
  11.5 21.2 %collective-permute-start = (bf16[256,1024]{1,0:T(8,128)(2,1)S(1)}, bf16[256,1024]{1,0:T(8,128)(2,1)S(1)}, u32[]{:S(2)}, u32[]{:S(2)}) collective-permute-start(bf16[256,1024]{1,0:T(8,128)(2,1)S(1)} %multiply_convert_fusion.2), channel_id=1, source_target_pairs={{0,4},{4,8},{8,12},{12,16},{16,20},{20,24},{24,28},{28,0},{1,5},{5... | collective-permute-start | bytes 1572872 | tf_op jit(solution)/shard_map/ppermute | solution.py:11
  32.7 25.0 %collective-permute-start.1 = (bf16[256,1024]{1,0:T(8,128)(2,1)S(1)}, bf16[256,1024]{1,0:T(8,128)(2,1)S(1)}, u32[]{:S(2)}, u32[]{:S(2)}) collective-permute-start(bf16[256,1024]{1,0:T(8,128)(2,1)S(1)} %collective-permute-done), channel_id=1, source_target_pairs={{0,4},{4,8},{8,12},{12,16},{16,20},{20,24},{24,28},{28,0},{1,5},{5... | collective-permute-start | bytes 1572872 | tf_op jit(solution)/shard_map/ppermute | solution.py:11
  57.7 26.8 %collective-permute-start.2 = (bf16[256,1024]{1,0:T(8,128)(2,1)S(1)}, bf16[256,1024]{1,0:T(8,128)(2,1)S(1)}, u32[]{:S(2)}, u32[]{:S(2)}) collective-permute-start(bf16[256,1024]{1,0:T(8,128)(2,1)S(1)} %collective-permute-done.1), channel_id=1, source_target_pairs={{0,4},{4,8},{8,12},{12,16},{16,20},{20,24},{24,28},{28,0},{1,5},{5... | collective-permute-start | bytes 1572872 | tf_op jit(solution)/shard_map/ppermute | solution.py:11
  84.6 26.9 %collective-permute-start.3 = (bf16[256,1024]{1,0:T(8,128)(2,1)S(1)}, bf16[256,1024]{1,0:T(8,128)(2,1)S(1)}, u32[]{:S(2)}, u32[]{:S(2)}) collective-permute-start(bf16[256,1024]{1,0:T(8,128)(2,1)S(1)} %collective-permute-done.2), channel_id=1, source_target_pairs={{0,4},{4,8},{8,12},{12,16},{16,20},{20,24},{24,28},{28,0},{1,5},{5... | collective-permute-start | bytes 1572872 | tf_op jit(solution)/shard_map/ppermute | solution.py:11
  111.5 18.0 %collective-permute-start.4 = (bf16[256,1024]{1,0:T(8,128)(2,1)S(1)}, bf16[256,1024]{1,0:T(8,128)(2,1)S(1)}, u32[]{:S(2)}, u32[]{:S(2)}) collective-permute-start(bf16[256,1024]{1,0:T(8,128)(2,1)S(1)} %collective-permute-done.3), channel_id=1, source_target_pairs={{0,4},{4,8},{8,12},{12,16},{16,20},{20,24},{24,28},{28,0},{1,5},{5... | collective-permute-start | bytes 1572872 | tf_op jit(solution)/shard_map/ppermute | solution.py:11
  129.5 0.8 copy-start.1
  130.3 14.2 %collective-permute-start.5 = (bf16[256,1024]{1,0:T(8,128)(2,1)S(1)}, bf16[256,1024]{1,0:T(8,128)(2,1)}, u32[]{:S(2)}, u32[]{:S(2)}) collective-permute-start(bf16[256,1024]{1,0:T(8,128)(2,1)S(1)} %collective-permute-done.4), channel_id=1, source_target_pairs={{0,4},{4,8},{8,12},{12,16},{16,20},{20,24},{24,28},{28,0},{1,5},{5... | collective-permute-start | bytes 1572872 | tf_op jit(solution)/shard_map/ppermute | solution.py:11
  144.5 13.6 %collective-permute-start.6 = (bf16[256,1024]{1,0:T(8,128)(2,1)}, bf16[256,1024]{1,0:T(8,128)(2,1)}, u32[]{:S(2)}, u32[]{:S(2)}) collective-permute-start(bf16[256,1024]{1,0:T(8,128)(2,1)} %collective-permute-done.5), channel_id=1, source_target_pairs={{0,4},{4,8},{8,12},{12,16},{16,20},{20,24},{24,28},{28,0},{1,5},{5... | collective-permute-start | bytes 1572872 | tf_op jit(solution)/shard_map/ppermute | solution.py:11
  144.5 57.7 %all-to-all-start = ((bf16[4,1024,512]{2,1,0:T(8,128)(2,1)}), bf16[4,1024,512]{2,1,0:T(8,128)(2,1)}, u32[]{:S(2)}, u32[]{:S(2)}) async-start(bf16[4,1024,512]{2,1,0:T(8,128)(2,1)} %bitcast.8), calls=%async_computation | async-start | bytes 8388608 | tf_op jit(solution)/shard_map/all_to_all | solution.py:17
  149.5 119.4 %reduce-scatter.2.cloned.1.call-start = ((), (), s32[]{:S(2)}) async-start(), calls=%async_computation.4 | async-start | bytes 5242880 | tf_op jit(solution)/shard_map/reduce_scatter | solution.py:25
  149.6 14.3 %copy-start.2 = (bf16[256,1024]{1,0:T(8,128)(2,1)S(1)}, bf16[256,1024]{1,0:T(8,128)(2,1)}, u32[]{:S(2)}) copy-start(bf16[256,1024]{1,0:T(8,128)(2,1)} %copy-done.1) | copy-start | bytes 1572868
Sparse Core Ops, SparseCore 0:
  10.7 104.7 all-gather.4
  117.0 46.3 all-gather.2
  223.4 45.4 reduce-scatter.1
